TPU v7x, 32 devices: a whole 2x2x4 slice. The times are simulated.
32 devices in a mesh: grp: 2 (over y), sp: 4 (over z), tp: 4 (over x, core).
Axes of the slice: x: 2, y: 2, z: 4, core: 2. Of those that a mesh axis runs over, the one named last changes fastest.
Arguments:
- stream: bfloat16 [2048, 4096], P(('grp', 'sp'), 'tp'), parts along dimension 0, may hold values from -6 to 6
- gain_pre: float32 [3, 4096], replicated, may hold values from 0.1 to 1.9
- w_in: bfloat16 [3, 4096, 1024], P(None, 'sp', 'tp'), may hold values from -0.09375 to 0.09375
- w_pool: bfloat16 [3, 4, 256, 256], P(None, 'tp'), may hold values from -0.375 to 0.375
- pool_scale: float32 [3, 1024], P(None, 'tp'), may hold values from 0.1 to 1.9
- w_out: bfloat16 [3, 1024, 4096], P(None, 'tp', 'sp'), may hold values from -0.5 to 0.5
- gain_post: float32 [3, 4096], replicated, may hold values from 0.1 to 1.9
Outputs:
- result: bfloat16 [2048, 4096], P(('grp', 'sp'), 'tp'), parts along dimension 0
There are 2 independent parts, one for each index of `grp`. A program takes and returns all parts, laid end to end along the dimension named above; an argument that names none is the same for every part. Nothing has to cross between parts.
All inputs are finite; a program needn't handle non-finite values.
Results may differ from a plain program's by a relative error of at most 0.02.
Values may be sent and summed in bfloat16 or wider, within the bound.
A program may use at most 64 MiB of HBM per device.

v0:
```python
import jax
import jax.numpy as jnp
from jax import lax
from jax.sharding import PartitionSpec as P

LAYERS = 3
WINDOWS = (2, 4, 8, 16)
EPS = 1e-06


def from_behind(block, axis, distance):
    devices = range(lax.axis_size(axis))
    route = [(i - distance, i) for i in devices if i - distance in devices]
    return lax.ppermute(block, axis, route)


def rms_scale(values, gain):
    inverse = lax.rsqrt(jnp.mean(values * values, axis=-1, keepdims=True) + EPS)
    return values * inverse * gain[None, :]


def per_device(stream, gain_pre, w_in, w_pool, pool_scale, w_out, gain_post):
    tok_rows = stream.shape[0]
    block_width = stream.shape[1]
    width = gain_pre.shape[1]
    group = w_pool.shape[2]
    reach = max(WINDOWS) - 1
    group_index = lax.axis_index("tp")
    window = jnp.where(
        group_index == 0, 2, jnp.where(group_index == 1, 4, jnp.where(group_index == 2, 8, 16))
    )
    positions = lax.axis_index("sp") * tok_rows + lax.iota(jnp.int32, tok_rows)
    count = jnp.minimum(positions + 1, window).astype(jnp.float32)
    gathered_in, gathered_out = (
        lax.all_gather(w_in, "sp", axis=1, tiled=True),
        lax.all_gather(w_out, "sp", axis=2, tiled=True),
    )
    current = stream
    feature_start = group_index * block_width
    for layer in range(LAYERS):
        full_rows = lax.all_gather(current, "tp", axis=1, tiled=True)
        normed = rms_scale(full_rows.astype(jnp.float32), gain_pre[layer]).astype(jnp.bfloat16)
        inner_sum = jnp.dot(normed, gathered_in[layer], preferred_element_type=jnp.float32)
        inner = inner_sum.astype(jnp.bfloat16)
        rim = from_behind(inner[tok_rows - reach :], "sp", 1)
        extended = jnp.concatenate([rim, inner], axis=0).astype(jnp.float32)
        summed = jnp.zeros((tok_rows, group), jnp.float32)
        for offset in range(max(WINDOWS)):
            window_slice = extended[reach - offset : reach - offset + tok_rows]
            summed = summed + jnp.where(offset < window, window_slice, 0.0)
        pooled = summed / count[:, None]
        spread = (pooled - inner.astype(jnp.float32)).astype(jnp.bfloat16)
        mixed = jnp.dot(spread, w_pool[layer, 0], preferred_element_type=jnp.float32)
        mixed = (mixed * pool_scale[layer][None, :]).astype(jnp.bfloat16)
        partial_value = jnp.dot(mixed, gathered_out[layer], preferred_element_type=jnp.float32)
        partial_value = partial_value.astype(jnp.bfloat16)
        branch = lax.psum_scatter(partial_value, "tp", scatter_dimension=1, tiled=True).astype(
            jnp.float32
        )
        squares = lax.psum(jnp.sum(branch * branch, axis=1), "tp")
        inverse = lax.rsqrt(squares / width + EPS)
        gain_block = lax.dynamic_slice_in_dim(gain_post[layer], feature_start, block_width, 0)
        normed_branch = branch * inverse[:, None] * gain_block[None, :]
        current = (current.astype(jnp.float32) + normed_branch).astype(jnp.bfloat16)
    return current


def solution(mesh):
    return jax.shard_map(
        per_device,
        mesh=mesh,
        in_specs=(
            P(("grp", "sp"), "tp"),
            P(),
            P(None, "sp", "tp"),
            P(None, "tp", None, None),
            P(None, "tp"),
            P(None, "tp", "sp"),
            P(),
        ),
        out_specs=P(("grp", "sp"), "tp"),
        check_vma=False,
    )
```

profile of v0, /device:TPU:0, one launch (start us, length us, event | category | flops | bytes accessed | tf_op | source)
XLA Modules:
  0.0 473.9 jit_solution(1717130798795279151)
XLA Ops:
  10.6 23.6 %all-gather.6.cloned.1.call-done = bf16[256,4096]{1,0:T(8,128)(2,1)} async-done(((bf16[256,1024]{1,0:T(8,128)(2,1)}), bf16[256,4096]{1,0:T(8,128)(2,1)}) %all-gather.6.cloned.1.call-update) | async-done | bytes 2097168 | tf_op jit(solution)/shard_map/all_gather | solution.py:41
  34.2 2.1 fusion
  36.3 114.8 %all-gather.8.cloned.1.call-done = bf16[3,4096,256]{2,1,0:T(8,128)(2,1)} async-done(((bf16[3,1024,256]{2,1,0:T(8,128)(2,1)}), bf16[3,4096,256]{2,1,0:T(8,128)(2,1)}) %all-gather.8.cloned.1.call-update) | async-done | bytes 6291472 | tf_op jit(solution)/shard_map/all_gather | solution.py:35
  151.1 3.0 fusion.24
  154.1 1.3 collective-permute-start
  155.5 1.3 collective-permute-done
  156.8 109.5 %all-gather.10.cloned.1.call-done = bf16[3,256,4096]{2,1,0:T(8,128)(2,1)} async-done(((bf16[3,256,1024]{2,1,0:T(8,128)(2,1)}), bf16[3,256,4096]{2,1,0:T(8,128)(2,1)}) %all-gather.10.cloned.1.call-update) | async-done | bytes 6291472 | tf_op jit(solution)/shard_map/all_gather | solution.py:36
  266.3 4.4 convolution_convert_fusion.2
  270.8 29.4 %reduce-scatter.4.cloned.1.call-done = bf16[256,1024]{1,0:T(8,128)(2,1)} async-done(((bf16[256,4096]{1,0:T(8,128)(2,1)}), bf16[256,1024]{1,0:T(8,128)(2,1)}) %reduce-scatter.4.cloned.1.call-update) | async-done | bytes 524304 | tf_op jit(solution)/shard_map/reduce_scatter | solution.py:57
  300.2 1.2 fusion.33
  301.4 5.8 %psum.21 = f32[256]{0:T(256)S(1)} all-reduce(f32[256]{0:T(256)S(1)} %fusion.33), channel_id=1, replica_groups=mesh['grp'=2,'sp'=4,'tp'=4] {'tp'}, use_global_device_ids=true, to_apply=%region_3.4 | all-reduce | flops 256 | bytes 2048 | tf_op jit(solution)/shard_map/psum | solution.py:60
  307.2 2.1 fusion.36
  309.4 23.3 %all-gather.12.cloned.1.call-done = bf16[256,4096]{1,0:T(8,128)(2,1)} async-done(((bf16[256,1024]{1,0:T(8,128)(2,1)}), bf16[256,4096]{1,0:T(8,128)(2,1)}) %all-gather.12.cloned.1.call-update) | async-done | bytes 2097168 | tf_op jit(solution)/shard_map/all_gather | solution.py:41
  332.7 2.1 fusion.3
  334.7 3.0 fusion.27
  337.8 3.4 collective-permute-start.1
  341.2 1.3 collective-permute-done.1
  342.5 4.4 convolution_convert_fusion.1
  347.0 32.0 %reduce-scatter.6.cloned.1.call-done = bf16[256,1024]{1,0:T(8,128)(2,1)} async-done(((bf16[256,4096]{1,0:T(8,128)(2,1)}), bf16[256,1024]{1,0:T(8,128)(2,1)}) %reduce-scatter.6.cloned.1.call-update) | async-done | bytes 524304 | tf_op jit(solution)/shard_map/reduce_scatter | solution.py:57
  379.0 1.2 fusion.37
  380.3 5.8 %psum.22 = f32[256]{0:T(256)S(1)} all-reduce(f32[256]{0:T(256)S(1)} %fusion.37), channel_id=1, replica_groups=mesh['grp'=2,'sp'=4,'tp'=4] {'tp'}, use_global_device_ids=true, to_apply=%region_7.8 | all-reduce | flops 256 | bytes 2048 | tf_op jit(solution)/shard_map/psum | solution.py:60
  386.0 2.1 fusion.40
  388.2 23.3 %all-gather.14.cloned.1.call-done = bf16[256,4096]{1,0:T(8,128)(2,1)} async-done(((bf16[256,1024]{1,0:T(8,128)(2,1)}), bf16[256,4096]{1,0:T(8,128)(2,1)}) %all-gather.14.cloned.1.call-update) | async-done | bytes 2097168 | tf_op jit(solution)/shard_map/all_gather | solution.py:41
  411.5 2.1 fusion.6
  413.6 3.0 fusion.30
  416.6 3.4 collective-permute-start.2
  420.0 1.3 collective-permute-done.2
  421.4 4.3 convolution_convert_fusion
  425.8 32.1 %reduce-scatter.8.cloned.1.call-done = bf16[256,1024]{1,0:T(8,128)(2,1)} async-done(((bf16[256,4096]{1,0:T(8,128)(2,1)}), bf16[256,1024]{1,0:T(8,128)(2,1)}) %reduce-scatter.8.cloned.1.call-update) | async-done | bytes 524304 | tf_op jit(solution)/shard_map/reduce_scatter | solution.py:57
  457.9 1.2 fusion.41
  459.1 5.8 %psum.23 = f32[256]{0:T(256)S(1)} all-reduce(f32[256]{0:T(256)S(1)} %fusion.41), channel_id=1, replica_groups=mesh['grp'=2,'sp'=4,'tp'=4] {'tp'}, use_global_device_ids=true, to_apply=%region_11.12 | all-reduce | flops 256 | bytes 2048 | tf_op jit(solution)/shard_map/psum | solution.py:60
  464.9 2.1 fusion.44
  (45 shorter events, 4.5 us)
Async XLA Ops:
  6.5 27.7 %all-gather.6.cloned.1.call-start = ((), (), s32[]{:S(2)}) async-start(), calls=%async_computation.3 | async-start | bytes 2621440 | tf_op jit(solution)/shard_map/all_gather | solution.py:41
  7.3 143.9 %all-gather.8.cloned.1.call-start = ((), (), s32[]{:S(2)}) async-start(), calls=%async_computation.4 | async-start | bytes 7864320 | tf_op jit(solution)/shard_map/all_gather | solution.py:35
  8.0 258.3 %all-gather.10.cloned.1.call-start = ((), (), s32[]{:S(2)}) async-start(), calls=%async_computation.5 | async-start | bytes 7864320 | tf_op jit(solution)/shard_map/all_gather | solution.py:36
  8.7 291.5 %reduce-scatter.4.cloned.1.call-start = ((), (), s32[]{:S(2)}) async-start(), calls=%async_computation.6 | async-start | bytes 2621440 | tf_op jit(solution)/shard_map/reduce_scatter | solution.py:57
  36.3 230.0 %copy-start.4 = (bf16[3,1,256,256]{3,2,1,0:T(8,128)(2,1)S(1)}, bf16[3,1,256,256]{3,2,1,0:T(8,128)(2,1)}, u32[]{:S(2)}) copy-start(bf16[3,1,256,256]{3,2,1,0:T(8,128)(2,1)} %param.10) | copy-start | bytes 1179652
  154.1 2.6 collective-permute-start
  266.3 4.4 copy-start.3
  266.3 40.9 %copy-start.2 = (bf16[256,1024]{1,0:T(8,128)(2,1)S(1)}, bf16[256,1024]{1,0:T(8,128)(2,1)}, u32[]{:S(2)}) copy-start(bf16[256,1024]{1,0:T(8,128)(2,1)} %param.7) | copy-start | bytes 1572868
  270.7 62.0 %all-gather.12.cloned.1.call-start = ((), (), s32[]{:S(2)}) async-start(), calls=%async_computation.7 | async-start | bytes 2621440 | tf_op jit(solution)/shard_map/all_gather | solution.py:41
  309.3 69.7 %reduce-scatter.6.cloned.1.call-start = ((), (), s32[]{:S(2)}) async-start(), calls=%async_computation.8 | async-start | bytes 2621440 | tf_op jit(solution)/shard_map/reduce_scatter | solution.py:57
  337.8 4.7 %collective-permute-start.1 = (bf16[15,256]{1,0:T(8,128)(2,1)S(1)}, bf16[15,256]{1,0:T(8,128)(2,1)S(1)}, u32[]{:S(2)}, u32[]{:S(2)}) collective-permute-start(bf16[15,256]{1,0:T(8,128)(2,1)S(1)} %slice.296), channel_id=1, source_target_pairs={{0,4},{4,8},{8,12},{1,5},{5,9},{9,13},{2,6},{6,10},{10,14},{3,7},{... | collective-permute-start | bytes 23048 | tf_op jit(solution)/shard_map/ppermute | solution.py:14
  342.5 43.5 %copy-start.1 = (bf16[256,1024]{1,0:T(8,128)(2,1)S(1)}, bf16[256,1024]{1,0:T(8,128)(2,1)}, u32[]{:S(2)}) copy-start(bf16[256,1024]{1,0:T(8,128)(2,1)} %fusion.36) | copy-start | bytes 1572868
  346.9 64.6 %all-gather.14.cloned.1.call-start = ((), (), s32[]{:S(2)}) async-start(), calls=%async_computation.9 | async-start | bytes 2621440 | tf_op jit(solution)/shard_map/all_gather | solution.py:41
  388.2 69.8 %reduce-scatter.8.cloned.1.call-start = ((), (), s32[]{:S(2)}) async-start(), calls=%async_computation.10 | async-start | bytes 2621440 | tf_op jit(solution)/shard_map/reduce_scatter | solution.py:57
  416.6 4.7 %collective-permute-start.2 = (bf16[15,256]{1,0:T(8,128)(2,1)S(1)}, bf16[15,256]{1,0:T(8,128)(2,1)S(1)}, u32[]{:S(2)}, u32[]{:S(2)}) collective-permute-start(bf16[15,256]{1,0:T(8,128)(2,1)S(1)} %slice.315), channel_id=1, source_target_pairs={{0,4},{4,8},{8,12},{1,5},{5,9},{9,13},{2,6},{6,10},{10,14},{3,7},{... | collective-permute-start | bytes 23048 | tf_op jit(solution)/shard_map/ppermute | solution.py:14
  421.4 43.5 %copy-start = (bf16[256,1024]{1,0:T(8,128)(2,1)S(1)}, bf16[256,1024]{1,0:T(8,128)(2,1)}, u32[]{:S(2)}) copy-start(bf16[256,1024]{1,0:T(8,128)(2,1)} %fusion.40) | copy-start | bytes 1572868
Sparse Core Ops, SparseCore 0:
  8.9 25.2 all-gather.5
  35.8 115.3 all-gather.7
  152.7 113.5 all-gather.9
  270.8 29.3 reduce-scatter.3
  309.4 23.1 all-gather.11
  347.1 31.9 reduce-scatter.5
  388.3 23.1 all-gather.13
  425.9 31.9 reduce-scatter.7
where the time goes:
time: 475 us; the launch traced here: 474 us
  waiting for transfers between devices  394 us (83%)
  matrix products  22 us (5%)
  blocking collectives  17.3 us (4%)
  other arithmetic  16.3 us (3%)
  between operations  13.7 us (3%)
  starting transfers between devices  8.35 us (2%)
    all_gather x1, waiting for transfers between devices, per_device(): lax.all_gather(w_in, 'sp', axis=1, tiled=True)  115 us
    all_gather x1, waiting for transfers between devices, per_device(): lax.all_gather(w_out, 'sp', axis=2, tiled=True)  109 us
    reduce_scatter x3, waiting for transfers between devices, per_device(): lax.psum_scatter(partial_value, 'tp', scatter_dimension=1, tiled=True)  93.6 us
    all_gather x3, waiting for transfers between devices, per_device(): full_rows = lax.all_gather(current, 'tp', axis=1, tiled=True)  70.2 us
    psum x3, blocking collectives, per_device(): squares = lax.psum(jnp.sum(branch * branch, axis=1), 'tp')  17.3 us
    dot_general x3, matrix products, per_device(): jnp.dot(mixed, gathered_out[layer], preferred_element_type=jnp.float32)  13.1 us
  transfers between devices with their start and end apart: 11, of which 11 were waited for; matrix products, arithmetic and copies ran while one was open for 1% of the time, Pallas kernels for 0%

commit v1 on v0

--- a/solution.py
+++ b/solution.py
@@ -38,7 +38,14 @@
     current = stream
     feature_start = group_index * block_width
     for layer in range(LAYERS):
-        full_rows = lax.all_gather(current, "tp", axis=1, tiled=True)
+        ring = [current]
+        for hop in range(3):
+            ring.append(lax.ppermute(ring[-1], "tp", [(dev, (dev + 1) % 4) for dev in range(4)]))
+        full_rows = jnp.roll(
+            jnp.concatenate(ring[::-1], axis=1),
+            (lax.axis_index("tp") + 1) * ring[0].shape[1],
+            axis=1,
+        )
         normed = rms_scale(full_rows.astype(jnp.float32), gain_pre[layer]).astype(jnp.bfloat16)
         inner_sum = jnp.dot(normed, gathered_in[layer], preferred_element_type=jnp.float32)
         inner = inner_sum.astype(jnp.bfloat16)

time: 475 us -> 457 us (0.962)
  waiting for transfers between devices: 394 us -> 374 us
    ppermute x0 -> x9, waiting for transfers between devices: none -> 76 us  [per_device(): lax.ppermute(ring[-1], 'tp', [(dev, (dev + 1) % 4) for dev in range(4)])]
    all_gather x3 -> x0, waiting for transfers between devices: 70.2 us -> none  [per_device(): full_rows = lax.all_gather(current, 'tp', axis=1, tiled=True)]
    all_gather x1, waiting for transfers between devices: 115 us -> 87.9 us  [per_device(): lax.all_gather(w_in, 'sp', axis=1, tiled=True)]
    reduce_sum x3, other arithmetic: 6.25 us -> 11.6 us  [rms_scale(): inverse = lax.rsqrt(jnp.mean(values * values, axis=-1, keepdims=True) + EPS)]
  transfers between devices with their start and end apart: 11 -> 17, of which waited for: 11 -> 17; matrix products, arithmetic and copies ran while one was open for 1% -> 2% of each run, Pallas kernels for 0% -> 0%
where the time goes in v1:
time: 457 us; the launch traced here: 456 us
  waiting for transfers between devices  374 us (82%)
  matrix products  20.2 us (4%)
  other arithmetic  20.1 us (4%)
  blocking collectives  17.3 us (4%)
  between operations  13.4 us (3%)
  starting transfers between devices  9.28 us (2%)
    all_gather x1, waiting for transfers between devices, per_device(): lax.all_gather(w_out, 'sp', axis=2, tiled=True)  110 us
    reduce_scatter x3, waiting for transfers between devices, per_device(): lax.psum_scatter(partial_value, 'tp', scatter_dimension=1, tiled=True)  94.5 us
    all_gather x1, waiting for transfers between devices, per_device(): lax.all_gather(w_in, 'sp', axis=1, tiled=True)  87.9 us
    ppermute x9, waiting for transfers between devices, per_device(): lax.ppermute(ring[-1], 'tp', [(dev, (dev + 1) % 4) for dev in range(4)])  76 us
    psum x3, blocking collectives, per_device(): squares = lax.psum(jnp.sum(branch * branch, axis=1), 'tp')  17.3 us
    dot_general x3, matrix products, per_device(): jnp.dot(mixed, gathered_out[layer], preferred_element_type=jnp.float32)  13 us
    reduce_sum x3, other arithmetic, rms_scale(): inverse = lax.rsqrt(jnp.mean(values * values, axis=-1, keepdims=True) + EPS)  11.6 us
  transfers between devices with their start and end apart: 17, of which 17 were waited for; matrix products, arithmetic and copies ran while one was open for 2% of the time, Pallas kernels for 0%

profile of v1, /device:TPU:0, one launch (start us, length us, event | category | flops | bytes accessed | tf_op | source)
XLA Modules:
  0.0 456.1 jit_solution(640396169059032821)
XLA Ops:
  8.6 9.0 %collective-permute-done = bf16[256,1024]{1,0:T(8,128)(2,1)S(1)} collective-permute-done((bf16[256,1024]{1,0:T(8,128)(2,1)}, bf16[256,1024]{1,0:T(8,128)(2,1)S(1)}, u32[]{:S(2)}, u32[]{:S(2)}) %collective-permute-start) | collective-permute-done | bytes 524320 | tf_op jit(solution)/shard_map/ppermute | solution.py:43
  17.6 8.6 %collective-permute-done.1 = bf16[256,1024]{1,0:T(8,128)(2,1)S(1)} collective-permute-done((bf16[256,1024]{1,0:T(8,128)(2,1)S(1)}, bf16[256,1024]{1,0:T(8,128)(2,1)S(1)}, u32[]{:S(2)}, u32[]{:S(2)}) %collective-permute-start.1) | collective-permute-done | bytes 524320 | tf_op jit(solution)/shard_map/ppermute | solution.py:43
  28.0 6.9 %collective-permute-done.2 = bf16[256,1024]{1,0:T(8,128)(2,1)} collective-permute-done((bf16[256,1024]{1,0:T(8,128)(2,1)S(1)}, bf16[256,1024]{1,0:T(8,128)(2,1)}, u32[]{:S(2)}, u32[]{:S(2)}) %collective-permute-start.2) | collective-permute-done | bytes 524320 | tf_op jit(solution)/shard_map/ppermute | solution.py:43
  34.9 4.2 fusion
  39.1 87.9 %all-gather.3.cloned.1.call-done = bf16[3,4096,256]{2,1,0:T(8,128)(2,1)} async-done(((bf16[3,1024,256]{2,1,0:T(8,128)(2,1)}), bf16[3,4096,256]{2,1,0:T(8,128)(2,1)}) %all-gather.3.cloned.1.call-update) | async-done | bytes 6291472 | tf_op jit(solution)/shard_map/all_gather | solution.py:35
  127.0 2.3 fusion.45
  130.7 1.3 collective-permute-done.3
  132.0 110.1 %all-gather.5.cloned.1.call-done = bf16[3,256,4096]{2,1,0:T(8,128)(2,1)} async-done(((bf16[3,256,1024]{2,1,0:T(8,128)(2,1)}), bf16[3,256,4096]{2,1,0:T(8,128)(2,1)}) %all-gather.5.cloned.1.call-update) | async-done | bytes 6291472 | tf_op jit(solution)/shard_map/all_gather | solution.py:36
  242.1 4.4 convolution_convert_fusion.2
  246.7 29.4 %reduce-scatter.4.cloned.1.call-done = bf16[256,1024]{1,0:T(8,128)(2,1)} async-done(((bf16[256,4096]{1,0:T(8,128)(2,1)}), bf16[256,1024]{1,0:T(8,128)(2,1)}) %reduce-scatter.4.cloned.1.call-update) | async-done | bytes 524304 | tf_op jit(solution)/shard_map/reduce_scatter | solution.py:64
  277.3 5.8 %psum.21 = f32[256]{0:T(256)S(1)} all-reduce(f32[256]{0:T(256)S(1)} %fusion.54), channel_id=1, replica_groups=mesh['grp'=2,'sp'=4,'tp'=4] {'tp'}, use_global_device_ids=true, to_apply=%region_3.5 | all-reduce | flops 256 | bytes 2048 | tf_op jit(solution)/shard_map/psum | solution.py:67
  284.4 8.6 %collective-permute-done.4 = bf16[256,1024]{1,0:T(8,128)(2,1)S(1)} collective-permute-done((bf16[256,1024]{1,0:T(8,128)(2,1)S(1)}, bf16[256,1024]{1,0:T(8,128)(2,1)S(1)}, u32[]{:S(2)}, u32[]{:S(2)}) %collective-permute-start.4) | collective-permute-done | bytes 524320 | tf_op jit(solution)/shard_map/ppermute | solution.py:43
  293.0 8.6 %collective-permute-done.5 = bf16[256,1024]{1,0:T(8,128)(2,1)S(1)} collective-permute-done((bf16[256,1024]{1,0:T(8,128)(2,1)S(1)}, bf16[256,1024]{1,0:T(8,128)(2,1)S(1)}, u32[]{:S(2)}, u32[]{:S(2)}) %collective-permute-start.5) | collective-permute-done | bytes 524320 | tf_op jit(solution)/shard_map/ppermute | solution.py:43
  301.6 8.6 %collective-permute-done.6 = bf16[256,1024]{1,0:T(8,128)(2,1)S(1)} collective-permute-done((bf16[256,1024]{1,0:T(8,128)(2,1)S(1)}, bf16[256,1024]{1,0:T(8,128)(2,1)S(1)}, u32[]{:S(2)}, u32[]{:S(2)}) %collective-permute-start.6) | collective-permute-done | bytes 524320 | tf_op jit(solution)/shard_map/ppermute | solution.py:43
  310.2 3.7 fusion.3
  314.0 2.4 fusion.48
  316.4 3.6 collective-permute-start.7
  320.0 1.3 collective-permute-done.7
  321.4 4.3 convolution_convert_fusion.1
  325.8 32.5 %reduce-scatter.6.cloned.1.call-done = bf16[256,1024]{1,0:T(8,128)(2,1)} async-done(((bf16[256,4096]{1,0:T(8,128)(2,1)}), bf16[256,1024]{1,0:T(8,128)(2,1)}) %reduce-scatter.6.cloned.1.call-update) | async-done | bytes 524304 | tf_op jit(solution)/shard_map/reduce_scatter | solution.py:64
  359.5 5.8 %psum.22 = f32[256]{0:T(256)S(1)} all-reduce(f32[256]{0:T(256)S(1)} %fusion.58), channel_id=1, replica_groups=mesh['grp'=2,'sp'=4,'tp'=4] {'tp'}, use_global_device_ids=true, to_apply=%region_7.9 | all-reduce | flops 256 | bytes 2048 | tf_op jit(solution)/shard_map/psum | solution.py:67
  366.7 8.6 %collective-permute-done.8 = bf16[256,1024]{1,0:T(8,128)(2,1)S(1)} collective-permute-done((bf16[256,1024]{1,0:T(8,128)(2,1)S(1)}, bf16[256,1024]{1,0:T(8,128)(2,1)S(1)}, u32[]{:S(2)}, u32[]{:S(2)}) %collective-permute-start.8) | collective-permute-done | bytes 524320 | tf_op jit(solution)/shard_map/ppermute | solution.py:43
  375.3 8.6 %collective-permute-done.9 = bf16[256,1024]{1,0:T(8,128)(2,1)S(1)} collective-permute-done((bf16[256,1024]{1,0:T(8,128)(2,1)S(1)}, bf16[256,1024]{1,0:T(8,128)(2,1)S(1)}, u32[]{:S(2)}, u32[]{:S(2)}) %collective-permute-start.9) | collective-permute-done | bytes 524320 | tf_op jit(solution)/shard_map/ppermute | solution.py:43
  383.9 8.6 %collective-permute-done.10 = bf16[256,1024]{1,0:T(8,128)(2,1)S(1)} collective-permute-done((bf16[256,1024]{1,0:T(8,128)(2,1)S(1)}, bf16[256,1024]{1,0:T(8,128)(2,1)S(1)}, u32[]{:S(2)}, u32[]{:S(2)}) %collective-permute-start.10) | collective-permute-done | bytes 524320 | tf_op jit(solution)/shard_map/ppermute | solution.py:43
  392.5 3.7 fusion.6
  396.2 2.4 fusion.51
  398.6 3.6 collective-permute-start.11
  402.2 1.3 collective-permute-done.11
  403.6 4.3 convolution_convert_fusion
  407.9 32.5 %reduce-scatter.8.cloned.1.call-done = bf16[256,1024]{1,0:T(8,128)(2,1)} async-done(((bf16[256,4096]{1,0:T(8,128)(2,1)}), bf16[256,1024]{1,0:T(8,128)(2,1)}) %reduce-scatter.8.cloned.1.call-update) | async-done | bytes 524304 | tf_op jit(solution)/shard_map/reduce_scatter | solution.py:64
  441.7 5.8 %psum.23 = f32[256]{0:T(256)S(1)} all-reduce(f32[256]{0:T(256)S(1)} %fusion.62), channel_id=1, replica_groups=mesh['grp'=2,'sp'=4,'tp'=4] {'tp'}, use_global_device_ids=true, to_apply=%region_11.13 | all-reduce | flops 256 | bytes 2048 | tf_op jit(solution)/shard_map/psum | solution.py:67
  447.4 2.1 fusion.65
  (50 shorter events, 11.9 us)
Async XLA Ops:
  6.5 120.4 %all-gather.3.cloned.1.call-start = ((), (), s32[]{:S(2)}) async-start(), calls=%async_computation.3 | async-start | bytes 7864320 | tf_op jit(solution)/shard_map/all_gather | solution.py:35
  7.3 234.8 %all-gather.5.cloned.1.call-start = ((), (), s32[]{:S(2)}) async-start(), calls=%async_computation.4 | async-start | bytes 7864320 | tf_op jit(solution)/shard_map/all_gather | solution.py:36
  8.0 268.1 %reduce-scatter.4.cloned.1.call-start = ((), (), s32[]{:S(2)}) async-start(), calls=%async_computation.5 | async-start | bytes 2621440 | tf_op jit(solution)/shard_map/reduce_scatter | solution.py:64
  8.1 9.5 %collective-permute-start = (bf16[256,1024]{1,0:T(8,128)(2,1)}, bf16[256,1024]{1,0:T(8,128)(2,1)S(1)}, u32[]{:S(2)}, u32[]{:S(2)}) collective-permute-start(bf16[256,1024]{1,0:T(8,128)(2,1)} %param.9), channel_id=1, source_target_pairs={{0,1},{1,2},{2,3},{3,0},{4,5},{5,6},{6,7},{7,4},{8,9},{9,10},{10,1... | collective-permute-start | bytes 1572872 | tf_op jit(solution)/shard_map/ppermute | solution.py:43
  17.6 8.6 %collective-permute-start.1 = (bf16[256,1024]{1,0:T(8,128)(2,1)S(1)}, bf16[256,1024]{1,0:T(8,128)(2,1)S(1)}, u32[]{:S(2)}, u32[]{:S(2)}) collective-permute-start(bf16[256,1024]{1,0:T(8,128)(2,1)S(1)} %collective-permute-done), channel_id=1, source_target_pairs={{0,1},{1,2},{2,3},{3,0},{4,5},{5,6},{6,7},{7,4},{8,9},{9,10},{10,1... | collective-permute-start | bytes 1572872 | tf_op jit(solution)/shard_map/ppermute | solution.py:43
  26.2 8.7 %collective-permute-start.2 = (bf16[256,1024]{1,0:T(8,128)(2,1)S(1)}, bf16[256,1024]{1,0:T(8,128)(2,1)}, u32[]{:S(2)}, u32[]{:S(2)}) collective-permute-start(bf16[256,1024]{1,0:T(8,128)(2,1)S(1)} %collective-permute-done.1), channel_id=1, source_target_pairs={{0,1},{1,2},{2,3},{3,0},{4,5},{5,6},{6,7},{7,4},{8,9},{9,10},{10,1... | collective-permute-start | bytes 1572872 | tf_op jit(solution)/shard_map/ppermute | solution.py:43
  129.3 2.6 collective-permute-start.3
  242.1 4.5 copy-start.1
  242.1 41.0 %copy-start = (bf16[256,1024]{1,0:T(8,128)(2,1)S(1)}, bf16[256,1024]{1,0:T(8,128)(2,1)}, u32[]{:S(2)}) copy-start(bf16[256,1024]{1,0:T(8,128)(2,1)} %param.9) | copy-start | bytes 1572868
  246.5 111.8 %reduce-scatter.6.cloned.1.call-start = ((), (), s32[]{:S(2)}) async-start(), calls=%async_computation.6 | async-start | bytes 2621440 | tf_op jit(solution)/shard_map/reduce_scatter | solution.py:64
  284.4 8.7 %collective-permute-start.4 = (bf16[256,1024]{1,0:T(8,128)(2,1)S(1)}, bf16[256,1024]{1,0:T(8,128)(2,1)S(1)}, u32[]{:S(2)}, u32[]{:S(2)}) collective-permute-start(bf16[256,1024]{1,0:T(8,128)(2,1)S(1)} %fusion.57), channel_id=1, source_target_pairs={{0,1},{1,2},{2,3},{3,0},{4,5},{5,6},{6,7},{7,4},{8,9},{9,10},{10,1... | collective-permute-start | bytes 1572872 | tf_op jit(solution)/shard_map/ppermute | solution.py:43
  293.0 8.6 %collective-permute-start.5 = (bf16[256,1024]{1,0:T(8,128)(2,1)S(1)}, bf16[256,1024]{1,0:T(8,128)(2,1)S(1)}, u32[]{:S(2)}, u32[]{:S(2)}) collective-permute-start(bf16[256,1024]{1,0:T(8,128)(2,1)S(1)} %collective-permute-done.4), channel_id=1, source_target_pairs={{0,1},{1,2},{2,3},{3,0},{4,5},{5,6},{6,7},{7,4},{8,9},{9,10},{10,1... | collective-permute-start | bytes 1572872 | tf_op jit(solution)/shard_map/ppermute | solution.py:43
  301.6 8.6 %collective-permute-start.6 = (bf16[256,1024]{1,0:T(8,128)(2,1)S(1)}, bf16[256,1024]{1,0:T(8,128)(2,1)S(1)}, u32[]{:S(2)}, u32[]{:S(2)}) collective-permute-start(bf16[256,1024]{1,0:T(8,128)(2,1)S(1)} %collective-permute-done.5), channel_id=1, source_target_pairs={{0,1},{1,2},{2,3},{3,0},{4,5},{5,6},{6,7},{7,4},{8,9},{9,10},{10,1... | collective-permute-start | bytes 1572872 | tf_op jit(solution)/shard_map/ppermute | solution.py:43
  313.9 7.4 %copy-start.2 = (bf16[3,1,256,256]{3,2,1,0:T(8,128)(2,1)S(1)}, bf16[3,1,256,256]{3,2,1,0:T(8,128)(2,1)}, u32[]{:S(2)}) copy-start(bf16[3,1,256,256]{3,2,1,0:T(8,128)(2,1)} %param.12) | copy-start | bytes 1179652
  316.4 4.9 %collective-permute-start.7 = (bf16[15,256]{1,0:T(8,128)(2,1)S(1)}, bf16[15,256]{1,0:T(8,128)(2,1)S(1)}, u32[]{:S(2)}, u32[]{:S(2)}) collective-permute-start(bf16[15,256]{1,0:T(8,128)(2,1)S(1)} %slice.296), channel_id=1, source_target_pairs={{0,4},{4,8},{8,12},{1,5},{5,9},{9,13},{2,6},{6,10},{10,14},{3,7},{... | collective-permute-start | bytes 23048 | tf_op jit(solution)/shard_map/ppermute | solution.py:14
  325.7 114.7 %reduce-scatter.8.cloned.1.call-start = ((), (), s32[]{:S(2)}) async-start(), calls=%async_computation.7 | async-start | bytes 2621440 | tf_op jit(solution)/shard_map/reduce_scatter | solution.py:64
  366.6 8.7 %collective-permute-start.8 = (bf16[256,1024]{1,0:T(8,128)(2,1)S(1)}, bf16[256,1024]{1,0:T(8,128)(2,1)S(1)}, u32[]{:S(2)}, u32[]{:S(2)}) collective-permute-start(bf16[256,1024]{1,0:T(8,128)(2,1)S(1)} %fusion.61), channel_id=1, source_target_pairs={{0,1},{1,2},{2,3},{3,0},{4,5},{5,6},{6,7},{7,4},{8,9},{9,10},{10,1... | collective-permute-start | bytes 1572872 | tf_op jit(solution)/shard_map/ppermute | solution.py:43
  375.3 8.6 %collective-permute-start.9 = (bf16[256,1024]{1,0:T(8,128)(2,1)S(1)}, bf16[256,1024]{1,0:T(8,128)(2,1)S(1)}, u32[]{:S(2)}, u32[]{:S(2)}) collective-permute-start(bf16[256,1024]{1,0:T(8,128)(2,1)S(1)} %collective-permute-done.8), channel_id=1, source_target_pairs={{0,1},{1,2},{2,3},{3,0},{4,5},{5,6},{6,7},{7,4},{8,9},{9,10},{10,1... | collective-permute-start | bytes 1572872 | tf_op jit(solution)/shard_map/ppermute | solution.py:43
  383.9 8.6 %collective-permute-start.10 = (bf16[256,1024]{1,0:T(8,128)(2,1)S(1)}, bf16[256,1024]{1,0:T(8,128)(2,1)S(1)}, u32[]{:S(2)}, u32[]{:S(2)}) collective-permute-start(bf16[256,1024]{1,0:T(8,128)(2,1)S(1)} %collective-permute-done.9), channel_id=1, source_target_pairs={{0,1},{1,2},{2,3},{3,0},{4,5},{5,6},{6,7},{7,4},{8,9},{9,10},{10,1... | collective-permute-start | bytes 1572872 | tf_op jit(solution)/shard_map/ppermute | solution.py:43
  398.6 4.9 %collective-permute-start.11 = (bf16[15,256]{1,0:T(8,128)(2,1)S(1)}, bf16[15,256]{1,0:T(8,128)(2,1)S(1)}, u32[]{:S(2)}, u32[]{:S(2)}) collective-permute-start(bf16[15,256]{1,0:T(8,128)(2,1)S(1)} %slice.315), channel_id=1, source_target_pairs={{0,4},{4,8},{8,12},{1,5},{5,9},{9,13},{2,6},{6,10},{10,14},{3,7},{... | collective-permute-start | bytes 23048 | tf_op jit(solution)/shard_map/ppermute | solution.py:14
Sparse Core Ops, SparseCore 0:
  8.9 118.0 all-gather.2
  128.6 113.5 all-gather.4
  246.7 29.3 reduce-scatter.3
  325.8 32.4 reduce-scatter.5
  408.0 32.3 reduce-scatter.7
